TPU v7x, 32 devices: a whole 2x2x4 slice. The times are simulated.
32 devices in a mesh: grp: 2 (over y), fs: 4 (over z), tp: 4 (over x, core).
Axes of the slice: x: 2, y: 2, z: 4, core: 2. Of those that a mesh axis runs over, the one named last changes fastest.
Arguments:
- tokens: bfloat16 [1536, 2048], P(('grp', 'tp')), parts along dimension 0, may hold values from -6 to 6
- routes: int32 [1536, 2], P(('grp', 'tp')), parts along dimension 0, may hold values from 0 to 3, all different within a row; in each aligned block of 192 rows (0 to 191, 192 to 383, ...) at most 128 rows name the same one
- route_weight: float32 [1536, 2], P(('grp', 'tp')), parts along dimension 0, may hold values from 0.2 to 1
- norm_gain: float32 [2048], P('fs'), may hold values from 0.1 to 1.9
- gate_train: float32 [4, 2048, 5632], P('tp', 'fs'), may hold values from -0.125 to 0.125
- up_train: float32 [4, 2048, 5632], P('tp', 'fs'), may hold values from -0.125 to 0.125
- down_train: float32 [4, 5632, 2048], P('tp', None, 'fs'), may hold values from -0.109375 to 0.109375
Outputs:
- gate_serve: bfloat16 [8, 2048, 5632], P(('grp', 'tp'), None, 'fs'), parts along dimension 0
- up_serve: bfloat16 [8, 2048, 5632], P(('grp', 'tp'), None, 'fs'), parts along dimension 0
- down_serve: bfloat16 [8, 5632, 2048], P(('grp', 'tp'), 'fs'), parts along dimension 0
- mixed: bfloat16 [1536, 2048], P(('grp', 'tp'), 'fs'), parts along dimension 0
There are 2 independent parts, one for each index of `grp`. A program takes and returns all parts, laid end to end along the dimension named above; an argument that names none is the same for every part. Nothing has to cross between parts.
Inputs may be any that keep to these rules, and one draw needn't show every extreme that they name: `routes`: each row names 2 different experts. In each aligned block of 192 rows no expert is named by more than 128 rows, a bound that some block reaches.
All inputs are finite; a program needn't handle non-finite values.
Results may differ from a plain program's by a relative error of at most 0.0087.
Values may be sent and summed in bfloat16 or wider, within the bound.
A program may use at most 128 MiB of HBM per device.

v0:
```python
import jax
import jax.numpy as jnp
from jax import lax
from jax.sharding import PartitionSpec as P

EXPERTS = 4
CAP = 128


def shards(tokens, routes, route_weight, norm_gain, gate_train, up_train, down_train):
    fs_count = lax.axis_size("fs")
    pieces = min(fs_count, 32)
    copies = fs_count // pieces
    gain_column = norm_gain[:, None]
    gate_low = (gate_train[0] * gain_column).astype(jnp.bfloat16)
    up_low = (up_train[0] * gain_column).astype(jnp.bfloat16)
    down_low = down_train[0].astype(jnp.bfloat16)
    gate_wide = jnp.tile(gate_low, (1, copies))
    up_wide = jnp.tile(up_low, (1, copies))
    down_wide = jnp.tile(down_low, (copies, 1))
    gate_new, up_new = (
        lax.all_to_all(gate_wide, "fs", split_axis=1, concat_axis=0, tiled=True),
        lax.all_to_all(up_wide, "fs", split_axis=1, concat_axis=0, tiled=True),
    )
    down_new = lax.all_to_all(down_wide, "fs", split_axis=0, concat_axis=1, tiled=True)
    tok_float = tokens.astype(jnp.float32)
    normed = (
        tok_float * lax.rsqrt(jnp.mean(tok_float * tok_float, axis=-1, keepdims=True) + 1e-06)
    ).astype(jnp.bfloat16)
    chosen = routes.reshape(-1)
    chosen_hot = (chosen[:, None] == jnp.arange(EXPERTS, dtype=jnp.int32)[None, :]).astype(
        jnp.int32
    )
    before = jnp.cumsum(chosen_hot, axis=0) - chosen_hot
    slot_rank = jnp.sum(before * chosen_hot, axis=1)
    slot_index = (chosen * CAP + slot_rank).reshape(routes.shape)
    slot_range = jnp.arange(EXPERTS * CAP, dtype=jnp.int32)
    select_rows = jnp.any(slot_range[:, None, None] == slot_index[None, :, :], axis=-1).astype(
        jnp.bfloat16
    )
    outgoing = jnp.dot(select_rows, normed, preferred_element_type=jnp.float32).astype(jnp.bfloat16)
    outgoing = outgoing.reshape(EXPERTS, CAP, normed.shape[1])
    arrived = lax.all_to_all(outgoing, "tp", split_axis=0, concat_axis=0, tiled=True).reshape(
        EXPERTS * CAP, normed.shape[1]
    )
    slot_count = EXPERTS * CAP // copies
    copy_index = lax.axis_index("fs") // pieces
    my_rows = lax.dynamic_slice_in_dim(arrived, copy_index * slot_count, slot_count, 0)
    gated = jnp.dot(my_rows, gate_new, preferred_element_type=jnp.float32)
    lifted = jnp.dot(my_rows, up_new, preferred_element_type=jnp.float32)
    hidden = (jax.nn.silu(gated) * lifted).astype(jnp.bfloat16)
    partial_out = jnp.dot(hidden, down_new, preferred_element_type=jnp.float32)
    placed = jnp.zeros((EXPERTS * CAP, partial_out.shape[1]), jnp.float32)
    placed = lax.dynamic_update_slice_in_dim(placed, partial_out, copy_index * slot_count, 0)
    expert_out = lax.psum_scatter(placed, "fs", scatter_dimension=1, tiled=True).astype(
        jnp.bfloat16
    )
    returned = lax.all_to_all(
        expert_out.reshape(EXPERTS, CAP, expert_out.shape[1]),
        "tp",
        split_axis=0,
        concat_axis=0,
        tiled=True,
    )
    returned = returned.reshape(EXPERTS * CAP, expert_out.shape[1]).astype(jnp.float32)
    blend_weight = jnp.sum(
        jnp.where(
            slot_range[None, None, :] == slot_index[:, :, None], route_weight[:, :, None], 0.0
        ),
        axis=1,
    )
    mixed = jnp.dot(
        blend_weight, returned, precision=lax.Precision.HIGHEST, preferred_element_type=jnp.float32
    )
    return (gate_new[None], up_new[None], down_new[None], mixed.astype(jnp.bfloat16))


def solution(mesh):
    in_specs = (
        P(("grp", "tp"), None),
        P(("grp", "tp"), None),
        P(("grp", "tp"), None),
        P("fs"),
        P("tp", "fs", None),
        P("tp", "fs", None),
        P("tp", None, "fs"),
    )
    out_specs = (
        P(("grp", "tp"), None, "fs"),
        P(("grp", "tp"), None, "fs"),
        P(("grp", "tp"), "fs", None),
        P(("grp", "tp"), "fs"),
    )
    return jax.shard_map(shards, mesh=mesh, in_specs=in_specs, out_specs=out_specs, check_vma=False)
```

profile of v0, /device:TPU:0, one launch (start us, length us, event | category | flops | bytes accessed | tf_op | source)
XLA Modules:
  0.0 587.4 jit_solution(4837379173826643466)
XLA Ops:
  7.2 0.8 copy.54
  8.3 1.2 reduce-window.6
  11.1 1.4 fusion.3
  12.4 3.3 convolution_convert_fusion
  15.7 4.2 all-to-all-start.3
  19.9 14.5 %squeeze.7 = f32[512,4,1408]{2,1,0:T(4,128)} reshape(f32[1,512,5632]{2,1,0:T(8,128)} %param.11) | data formatting | bytes 23068672 | tf_op jit(solution)/shard_map/squeeze | solution.py:15
  34.5 14.5 %squeeze.8 = f32[512,4,1408]{2,1,0:T(4,128)} reshape(f32[1,512,5632]{2,1,0:T(8,128)} %param.12) | data formatting | bytes 23068672 | tf_op jit(solution)/shard_map/squeeze | solution.py:16
  49.0 16.8 %fusion = (bf16[512,4,1408]{2,0,1:T(8,128)(2,1)}, bf16[512,4,1408]{2,0,1:T(8,128)(2,1)}) fusion(f32[512,4,1408]{2,1,0:T(4,128)} %squeeze.8, f32[512]{0:T(512)S(1)} %copy-done, f32[512,4,1408]{2,1,0:T(4,128)} %squeeze.7), kind=kLoop, calls=%fused_computation.1 | loop fusion | flops 11534336 | bytes 34605056 | tf_op jit(solution)/shard_map/convert_element_type | solution.py:16
  65.9 5.7 all-to-all-start
  71.6 7.5 %convert_element_type.44 = bf16[1,5632,512]{2,1,0:T(8,128)(2,1)} convert(f32[1,5632,512]{2,1,0:T(8,128)} %param.13) | non-fusion elementwise | flops 2883584 | bytes 17301504 | tf_op jit(solution)/shard_map/convert_element_type | solution.py:17
  79.1 120.5 %all-to-all-done = bf16[512,4,1408]{2,0,1:T(8,128)(2,1)} async-done(((bf16[512,4,1408]{2,0,1:T(8,128)(2,1)}), bf16[512,4,1408]{2,0,1:T(8,128)(2,1)}, u32[]{:S(2)}, u32[]{:S(2)}) %all-to-all-start) | async-done | bytes 5767200 | tf_op jit(solution)/shard_map/all_to_all | solution.py:22
  199.6 133.5 %all_to_all.58 = bf16[4,1408,512]{2,1,0:T(8,128)(2,1)} all-to-all(bf16[4,1408,512]{2,1,0:T(8,128)(2,1)} %bitcast.49), channel_id=1, replica_groups=mesh['grp'=2,'fs'=4,'tp'=4] {'fs'}, dimensions={0} | all-to-all | bytes 11534336 | tf_op jit(solution)/shard_map/all_to_all | solution.py:25
  333.2 5.2 all-to-all-start.1
  338.6 8.3 %copy.53 = bf16[4,1408,512]{1,2,0:T(8,128)(2,1)} copy(bf16[4,1408,512]{2,1,0:T(8,128)(2,1)} %all_to_all.58) | data formatting | bytes 11534336 | tf_op jit(solution)/shard_map/all_to_all | solution.py:25
  346.9 7.6 %fusion.14 = f32[512,1408]{1,0:T(8,128)} fusion(bf16[512,2048]{1,0:T(8,128)(2,1)S(1)} %bitcast.50, bf16[2048,1408]{1,0:T(8,128)(2,1)} %bitcast.10), kind=kOutput, calls=%fused_computation.30 | convolution fusion | flops 2952790016 | bytes 10747904 | tf_op jit(solution)/shard_map/dot_general | solution.py:49
  354.5 110.3 %all-to-all-done.1 = bf16[512,4,1408]{2,0,1:T(8,128)(2,1)} async-done(((bf16[512,4,1408]{2,0,1:T(8,128)(2,1)}), bf16[512,4,1408]{2,0,1:T(8,128)(2,1)}, u32[]{:S(2)}, u32[]{:S(2)}) %all-to-all-start.1) | async-done | bytes 5767200 | tf_op jit(solution)/shard_map/all_to_all | solution.py:23
  464.8 13.9 %fusion.8 = f32[512,2048]{1,0:T(8,128)} fusion(bf16[1408,2048]{0,1:T(8,128)(2,1)} %bitcast.47, bf16[512,2048]{1,0:T(8,128)(2,1)S(1)} %bitcast.51, bf16[2048,1408]{1,0:T(8,128)(2,1)} %bitcast.11, f32[512,1408]{1,0:T(8,128)} %fusion.14), kind=kOutput, calls=%fused_computation.17 | convolution fusion | flops 5909905408 | bytes 20709376 | tf_op jit(solution)/shard_map/dot_general | solution.py:52
  478.7 75.2 %reduce-scatter.2.cloned.1.call-done = f32[512,512]{1,0:T(8,128)} async-done(((f32[512,2048]{1,0:T(8,128)}), f32[512,512]{1,0:T(8,128)}) %reduce-scatter.2.cloned.1.call-update) | async-done | bytes 1048592 | tf_op jit(solution)/shard_map/reduce_scatter | solution.py:55
  553.9 2.1 convert_element_type.52
  555.9 3.5 all-to-all-start.4
  559.6 8.2 %copy.57 = bf16[1,1408,2048]{2,1,0:T(8,128)(2,1)} copy(bf16[1,1408,2048]{1,2,0:T(8,128)(2,1)} %bitcast.48) | data formatting | bytes 11534336
  568.2 1.2 convolution_convert_fusion.1
  569.4 5.6 copy.68
  575.0 5.6 copy.69
  (21 shorter events, 2.6 us)
Async XLA Ops:
  15.7 50.1 %all-to-all-start.3 = ((bf16[4,128,2048]{2,1,0:T(8,128)(2,1)}), bf16[4,128,2048]{2,1,0:T(8,128)(2,1)S(1)}, u32[]{:S(2)}, u32[]{:S(2)}) async-start(bf16[4,128,2048]{2,1,0:T(8,128)(2,1)} %bitcast.8), calls=%async_computation.3 | async-start | bytes 4194304 | tf_op jit(solution)/shard_map/all_to_all | solution.py:43
  34.5 14.5 %copy-start = (f32[512]{0:T(512)S(1)}, f32[512]{0:T(512)}, u32[]{:S(2)}) copy-start(f32[512]{0:T(512)} %param.10) | copy-start | bytes 6148
  65.9 133.8 %all-to-all-start = ((bf16[512,4,1408]{2,0,1:T(8,128)(2,1)}), bf16[512,4,1408]{2,0,1:T(8,128)(2,1)}, u32[]{:S(2)}, u32[]{:S(2)}) async-start(bf16[512,4,1408]{2,0,1:T(8,128)(2,1)} %get-tuple-element.17), calls=%async_computation | async-start | bytes 11534336 | tf_op jit(solution)/shard_map/all_to_all | solution.py:22
  333.2 131.6 %all-to-all-start.1 = ((bf16[512,4,1408]{2,0,1:T(8,128)(2,1)}), bf16[512,4,1408]{2,0,1:T(8,128)(2,1)}, u32[]{:S(2)}, u32[]{:S(2)}) async-start(bf16[512,4,1408]{2,0,1:T(8,128)(2,1)} %get-tuple-element.16), calls=%async_computation.1 | async-start | bytes 11534336 | tf_op jit(solution)/shard_map/all_to_all | solution.py:23
  338.3 215.5 %reduce-scatter.2.cloned.1.call-start = ((), (), s32[]{:S(2)}) async-start(), calls=%async_computation.6 | async-start | bytes 5242880 | tf_op jit(solution)/shard_map/reduce_scatter | solution.py:55
  478.7 80.8 %copy-start.1 = (f32[192,2]{0,1:T(2,128)S(1)}, f32[192,2]{0,1:T(2,128)}, u32[]{:S(2)}) copy-start(f32[192,2]{0,1:T(2,128)} %param.9) | copy-start | bytes 4612
  555.9 12.3 %all-to-all-start.4 = ((bf16[4,128,512]{2,1,0:T(8,128)(2,1)}), bf16[4,128,512]{2,1,0:T(8,128)(2,1)S(1)}, u32[]{:S(2)}, u32[]{:S(2)}) async-start(bf16[4,128,512]{2,1,0:T(8,128)(2,1)} %bitcast.13), calls=%async_computation.5 | async-start | bytes 1048576 | tf_op jit(solution)/shard_map/all_to_all | solution.py:58
Sparse Core Ops, SparseCore 0:
  478.8 74.9 reduce-scatter.1
where the time goes:
time: 589 us; the launch traced here: 587 us
  waiting for transfers between devices  306 us (52%)
  blocking collectives  134 us (23%)
  local copies, waits for them, and re-layouts  58.3 us (10%)
  other arithmetic  30.4 us (5%)
  matrix products  25.9 us (4%)
  starting transfers between devices  18.8 us (3%)
  between operations  14.1 us (2%)
    all_to_all x1, blocking collectives, shards(): lax.all_to_all(down_wide, 'fs', split_axis=0, concat_axis=1, tiled=True)  134 us
    all_to_all x1, waiting for transfers between devices, shards(): lax.all_to_all(gate_wide, 'fs', split_axis=1, concat_axis=0, tiled=True)  120 us
    all_to_all x1, waiting for transfers between devices, shards(): lax.all_to_all(up_wide, 'fs', split_axis=1, concat_axis=0, tiled=True)  110 us
    reduce_scatter x1, waiting for transfers between devices, shards(): lax.psum_scatter(placed, 'fs', scatter_dimension=1, tiled=True)  75.2 us
    unnamed x8, local copies, waits for them, and re-layouts  20.2 us
    convert_element_type x1, other arithmetic, shards(): up_low = (up_train[0] * gain_column).astype(jnp.bfloat16)  16.8 us
    squeeze x1, local copies, waits for them, and re-layouts, shards(): gate_low = (gate_train[0] * gain_column).astype(jnp.bfloat16)  14.5 us
    squeeze x1, local copies, waits for them, and re-layouts, shards(): up_low = (up_train[0] * gain_column).astype(jnp.bfloat16)  14.5 us
  transfers between devices with their start and end apart: 5, of which 4 were waited for; matrix products, arithmetic and copies ran while one was open for 13% of the time, Pallas kernels for 0%

commit v1 on v0

--- a/solution.py
+++ b/solution.py
@@ -5,6 +5,12 @@
 
 EXPERTS = 4
 CAP = 128
+
+
+def swap_blocks(x, mesh_axis, split, join):
+    pieces = jnp.split(x, lax.axis_size(mesh_axis), axis=split)
+    got = lax.all_to_all(jnp.stack(pieces), mesh_axis, 0, 0)
+    return jnp.concatenate(got, axis=join)
 
 
 def shards(tokens, routes, route_weight, norm_gain, gate_train, up_train, down_train):
@@ -22,7 +28,7 @@
         lax.all_to_all(gate_wide, "fs", split_axis=1, concat_axis=0, tiled=True),
         lax.all_to_all(up_wide, "fs", split_axis=1, concat_axis=0, tiled=True),
     )
-    down_new = lax.all_to_all(down_wide, "fs", split_axis=0, concat_axis=1, tiled=True)
+    down_new = swap_blocks(down_wide, "fs", 0, 1)
     tok_float = tokens.astype(jnp.float32)
     normed = (
         tok_float * lax.rsqrt(jnp.mean(tok_float * tok_float, axis=-1, keepdims=True) + 1e-06)

time: 589 us -> 590 us (level)
    unnamed x8 -> x9, local copies, waits for them, and re-layouts: 20.2 us -> 29.8 us
    all_to_all x1 -> x0, local copies, waits for them, and re-layouts: 8.34 us -> none  [shards(): lax.all_to_all(down_wide, 'fs', split_axis=0, concat_axis=1, tiled=True)]
    convert_element_type x1 -> x0, other arithmetic: 7.55 us -> none  [shards(): down_low = down_train[0].astype(jnp.bfloat16)]
where the time goes in v1:
time: 590 us; the launch traced here: 588 us
  waiting for transfers between devices  306 us (52%)
  blocking collectives  135 us (23%)
  local copies, waits for them, and re-layouts  62.7 us (11%)
  other arithmetic  26.1 us (4%)
  matrix products  25.9 us (4%)
  starting transfers between devices  18.2 us (3%)
  between operations  14.1 us (2%)
    all_to_all x1, blocking collectives, shards(): lax.all_to_all(gate_wide, 'fs', split_axis=1, concat_axis=0, tiled=True)  135 us
    all_to_all x1, waiting for transfers between devices, swap_blocks(): got = lax.all_to_all(jnp.stack(pieces), mesh_axis, 0, 0)  119 us
    all_to_all x1, waiting for transfers between devices, shards(): lax.all_to_all(up_wide, 'fs', split_axis=1, concat_axis=0, tiled=True)  111 us
    reduce_scatter x1, waiting for transfers between devices, shards(): lax.psum_scatter(placed, 'fs', scatter_dimension=1, tiled=True)  75.6 us
    unnamed x9, local copies, waits for them, and re-layouts  29.8 us
    convert_element_type x1, other arithmetic, shards(): up_low = (up_train[0] * gain_column).astype(jnp.bfloat16)  16.8 us
    squeeze x1, local copies, waits for them, and re-layouts, shards(): gate_low = (gate_train[0] * gain_column).astype(jnp.bfloat16)  14.5 us
    squeeze x1, local copies, waits for them, and re-layouts, shards(): up_low = (up_train[0] * gain_column).astype(jnp.bfloat16)  14.5 us
  transfers between devices with their start and end apart: 5, of which 4 were waited for; matrix products, arithmetic and copies ran while one was open for 13% of the time, Pallas kernels for 0%

profile of v1, /device:TPU:0, one launch (start us, length us, event | category | flops | bytes accessed | tf_op | source)
XLA Modules:
  0.0 588.0 jit_solution(3417720503515890875)
XLA Ops:
  8.3 1.2 reduce-window.6
  11.1 1.4 fusion.3
  12.4 3.3 convolution_convert_fusion
  15.7 4.2 all-to-all-start.3
  19.9 14.5 %squeeze.8 = f32[512,4,1408]{2,1,0:T(4,128)} reshape(f32[1,512,5632]{2,1,0:T(8,128)} %param.12) | data formatting | bytes 23068672 | tf_op jit(solution)/shard_map/squeeze | solution.py:22
  34.5 14.5 %squeeze.7 = f32[512,4,1408]{2,1,0:T(4,128)} reshape(f32[1,512,5632]{2,1,0:T(8,128)} %param.11) | data formatting | bytes 23068672 | tf_op jit(solution)/shard_map/squeeze | solution.py:21
  49.0 16.8 %fusion = (bf16[512,4,1408]{2,0,1:T(8,128)(2,1)}, bf16[512,4,1408]{2,0,1:T(8,128)(2,1)}) fusion(f32[512,4,1408]{2,1,0:T(4,128)} %squeeze.8, f32[512]{0:T(512)S(1)} %copy-done, f32[512,4,1408]{2,1,0:T(4,128)} %squeeze.7), kind=kLoop, calls=%fused_computation.1 | loop fusion | flops 11534336 | bytes 34605056 | tf_op jit(solution)/shard_map/convert_element_type | solution.py:22
  65.9 135.1 %all_to_all.47 = bf16[512,4,1408]{2,0,1:T(8,128)(2,1)} all-to-all(bf16[512,4,1408]{2,0,1:T(8,128)(2,1)} %get-tuple-element.21), channel_id=1, replica_groups=mesh['grp'=2,'fs'=4,'tp'=4] {'fs'}, dimensions={1} | all-to-all | bytes 11534336 | tf_op jit(solution)/shard_map/all_to_all | solution.py:28
  200.9 5.2 all-to-all-start.1
  206.1 9.6 %copy.38 = bf16[1,5632,512]{1,2,0:T(8,128)(2,1)} copy(f32[1,5632,512]{2,1,0:T(8,128)} %param.13) | data formatting | bytes 17301504 | tf_op args[6]
  215.6 3.1 fusion.14
  218.8 3.2 pad_maximum_fusion
  222.0 111.3 %all-to-all-done.1 = bf16[512,4,1408]{2,0,1:T(8,128)(2,1)} async-done(((bf16[512,4,1408]{2,0,1:T(8,128)(2,1)}), bf16[512,4,1408]{2,0,1:T(8,128)(2,1)}, u32[]{:S(2)}, u32[]{:S(2)}) %all-to-all-start.1) | async-done | bytes 5767200 | tf_op jit(solution)/shard_map/all_to_all | solution.py:29
  333.3 5.2 all-to-all-start.2
  338.7 7.6 %fusion.15 = f32[512,1408]{1,0:T(8,128)} fusion(bf16[512,2048]{1,0:T(8,128)(2,1)S(1)} %bitcast.48, bf16[2048,1408]{1,0:T(8,128)(2,1)} %bitcast.46), kind=kOutput, calls=%fused_computation.32 | convolution fusion | flops 2952790016 | bytes 10747904 | tf_op jit(solution)/shard_map/dot_general | solution.py:55
  346.3 118.6 %all-to-all-done.2 = bf16[4,1408,512]{1,2,0:T(8,128)(2,1)} async-done(((bf16[4,1408,512]{1,2,0:T(8,128)(2,1)}), bf16[4,1408,512]{1,2,0:T(8,128)(2,1)}, u32[]{:S(2)}, u32[]{:S(2)}) %all-to-all-start.2) | async-done | bytes 5767200 | tf_op jit(solution)/shard_map/all_to_all | solution.py:12
  464.9 13.9 %fusion.8 = f32[512,2048]{1,0:T(8,128)} fusion(bf16[1408,2048]{0,1:T(8,128)(2,1)} %bitcast.11, bf16[512,2048]{1,0:T(8,128)(2,1)S(1)} %bitcast.49, bf16[2048,1408]{1,0:T(8,128)(2,1)} %bitcast.10, f32[512,1408]{1,0:T(8,128)} %fusion.15), kind=kOutput, calls=%fused_computation.18 | convolution fusion | flops 5909905408 | bytes 20709376 | tf_op jit(solution)/shard_map/dot_general | solution.py:58
  478.8 75.6 %reduce-scatter.2.cloned.1.call-done = f32[512,512]{1,0:T(8,128)} async-done(((f32[512,2048]{1,0:T(8,128)}), f32[512,512]{1,0:T(8,128)}) %reduce-scatter.2.cloned.1.call-update) | async-done | bytes 1048592 | tf_op jit(solution)/shard_map/reduce_scatter | solution.py:61
  554.4 2.1 convert_element_type.48
  556.5 3.5 all-to-all-start.4
  560.2 8.2 %copy.42 = bf16[1,1408,2048]{2,1,0:T(8,128)(2,1)} copy(bf16[1,1408,2048]{1,2,0:T(8,128)(2,1)} %bitcast.5) | data formatting | bytes 11534336
  568.8 1.2 convolution_convert_fusion.1
  569.9 5.6 copy.53
  575.5 5.6 copy.54
  (22 shorter events, 3.4 us)
Async XLA Ops:
  15.7 50.1 %all-to-all-start.3 = ((bf16[4,128,2048]{2,1,0:T(8,128)(2,1)}), bf16[4,128,2048]{2,1,0:T(8,128)(2,1)S(1)}, u32[]{:S(2)}, u32[]{:S(2)}) async-start(bf16[4,128,2048]{2,1,0:T(8,128)(2,1)} %bitcast.7), calls=%async_computation.3 | async-start | bytes 4194304 | tf_op jit(solution)/shard_map/all_to_all | solution.py:49
  34.5 14.5 %copy-start = (f32[512]{0:T(512)S(1)}, f32[512]{0:T(512)}, u32[]{:S(2)}) copy-start(f32[512]{0:T(512)} %param.10) | copy-start | bytes 6148
  200.9 132.4 %all-to-all-start.1 = ((bf16[512,4,1408]{2,0,1:T(8,128)(2,1)}), bf16[512,4,1408]{2,0,1:T(8,128)(2,1)}, u32[]{:S(2)}, u32[]{:S(2)}) async-start(bf16[512,4,1408]{2,0,1:T(8,128)(2,1)} %get-tuple-element.20), calls=%async_computation.1 | async-start | bytes 11534336 | tf_op jit(solution)/shard_map/all_to_all | solution.py:29
  333.3 131.6 %all-to-all-start.2 = ((bf16[4,1408,512]{1,2,0:T(8,128)(2,1)}), bf16[4,1408,512]{1,2,0:T(8,128)(2,1)}, u32[]{:S(2)}, u32[]{:S(2)}) async-start(bf16[4,1408,512]{1,2,0:T(8,128)(2,1)} %pad_maximum_fusion), calls=%async_computation.2 | async-start | bytes 11534336 | tf_op jit(solution)/shard_map/all_to_all | solution.py:12
  338.5 216.0 %reduce-scatter.2.cloned.1.call-start = ((), (), s32[]{:S(2)}) async-start(), calls=%async_computation.6 | async-start | bytes 5242880 | tf_op jit(solution)/shard_map/reduce_scatter | solution.py:61
  478.8 81.2 %copy-start.1 = (f32[192,2]{0,1:T(2,128)S(1)}, f32[192,2]{0,1:T(2,128)}, u32[]{:S(2)}) copy-start(f32[192,2]{0,1:T(2,128)} %param.9) | copy-start | bytes 4612
  556.5 12.3 %all-to-all-start.4 = ((bf16[4,128,512]{2,1,0:T(8,128)(2,1)}), bf16[4,128,512]{2,1,0:T(8,128)(2,1)S(1)}, u32[]{:S(2)}, u32[]{:S(2)}) async-start(bf16[4,128,512]{2,1,0:T(8,128)(2,1)} %bitcast.12), calls=%async_computation.5 | async-start | bytes 1048576 | tf_op jit(solution)/shard_map/all_to_all | solution.py:64
Sparse Core Ops, SparseCore 0:
  479.0 75.4 reduce-scatter.1
